TPU v7x, 32 devices: a whole 2x2x4 slice. The times are simulated.
32 devices in a mesh: ep: 8 (over z, core), tp: 4 (over y, x).
Axes of the slice: x: 2, y: 2, z: 4, core: 2. Of those that a mesh axis runs over, the one named last changes fastest.
Arguments:
- tokens: bfloat16 [256, 2560], P('ep'), may hold values from -6 to 6
- norm_gain: float32 [2560], replicated, may hold values from 0.1 to 1.9
- route: int32 [256, 4], P('ep'), may hold values from 0 to 7, all different within a row; in each aligned block of 32 rows (0 to 31, 32 to 63, ...) at most 24 rows name the same one
- route_weight: float32 [256, 4], P('ep'), may hold values from 0.1 to 1
- gate_weight: bfloat16 [8, 8960, 2560], P('ep', 'tp'), may hold values from -0.125 to 0.125
- up_weight: bfloat16 [8, 8960, 2560], P('ep', 'tp'), may hold values from -0.125 to 0.125
- down_weight: bfloat16 [8, 8960, 2560], P('ep', 'tp'), may hold values from -0.0625 to 0.0625
Outputs:
- mixed: bfloat16 [256, 2560], P('ep', 'tp')
Inputs may be any that keep to these rules, and one draw needn't show every extreme that they name: `route`: each row names 4 different experts. Among the rows of one index of ep no expert is named more than 24 times, a bound that some block reaches.
All inputs are finite; a program needn't handle non-finite values.
Results may differ from a plain program's by a relative error of at most 0.018.
Values may be sent and summed in bfloat16 or wider, within the bound.
A program may use at most 128 MiB of HBM per device.

v0:
```python
import jax
import jax.numpy as jnp
from jax import lax
from jax.sharding import PartitionSpec as P

epsilon = 1e-06


def on_device(tokens, norm_gain, route, route_weight, gate_weight, up_weight, down_weight):
    tok_rows, width = tokens.shape
    top_count = route.shape[1]
    local_experts = gate_weight.shape[0]
    ep_count = lax.axis_size("ep")
    tp_count = lax.axis_size("tp")
    experts = local_experts * ep_count
    capacity = min(tok_rows, max(2, (3 * tok_rows * top_count + 2 * experts - 1) // (2 * experts)))
    width_share = width // tp_count
    values = tokens.astype(jnp.float32)
    scaled = values * lax.rsqrt(jnp.mean(values * values, axis=-1, keepdims=True) + epsilon)
    normed = (scaled * norm_gain).astype(jnp.bfloat16)
    flat_route = route.reshape(tok_rows * top_count)
    onehot = (flat_route[:, None] == jnp.arange(experts, dtype=jnp.int32)[None, :]).astype(
        jnp.int32
    )
    slot_number = jnp.sum((jnp.cumsum(onehot, axis=0) - 1) * onehot, axis=-1)
    slot_index = flat_route * capacity + slot_number
    placing = (
        slot_index[None, :] == jnp.arange(experts * capacity, dtype=jnp.int32)[:, None]
    ).astype(jnp.bfloat16)
    repeated = jnp.repeat(normed, top_count, axis=0)
    columns = lax.dynamic_slice_in_dim(repeated, lax.axis_index("tp") * width_share, width_share, 1)
    send = jnp.dot(placing, columns, preferred_element_type=jnp.float32).astype(jnp.bfloat16)
    send = send.reshape(ep_count, local_experts, capacity, width_share)
    arrived = lax.all_to_all(send, "ep", split_axis=0, concat_axis=0, tiled=True)
    piece = lax.all_gather(arrived, "tp", axis=3, tiled=True)
    gate = jnp.einsum("sjcd,jfd->sjcf", piece, gate_weight, preferred_element_type=jnp.float32)
    upward = jnp.einsum("sjcd,jfd->sjcf", piece, up_weight, preferred_element_type=jnp.float32)
    hidden = (jax.nn.silu(gate) * upward).astype(jnp.bfloat16)
    partial_value = jnp.einsum(
        "sjcf,jfd->sjcd", hidden, down_weight, preferred_element_type=jnp.float32
    )
    shares = lax.psum_scatter(
        partial_value.astype(jnp.bfloat16), "tp", scatter_dimension=3, tiled=True
    )
    returned = lax.all_to_all(shares, "ep", split_axis=0, concat_axis=0, tiled=True)
    results = returned.reshape(experts * capacity, width_share)
    picked = results[slot_index].reshape(tok_rows, top_count, width_share).astype(jnp.float32)
    mixed = jnp.sum(route_weight[:, :, None] * picked, axis=1)
    return mixed.astype(jnp.bfloat16)


def solution(mesh):
    placed = (
        P("ep", None),
        P(),
        P("ep", None),
        P("ep", None),
        P("ep", "tp", None),
        P("ep", "tp", None),
        P("ep", "tp", None),
    )
    return jax.shard_map(
        on_device, mesh=mesh, in_specs=placed, out_specs=P("ep", "tp"), check_vma=False
    )
```

profile of v0, /device:TPU:0, one launch (start us, length us, event | category | flops | bytes accessed | tf_op | source)
XLA Modules:
  0.0 130.7 jit_solution(8233798995752015378)
XLA Ops:
  6.5 0.8 copy.15
  7.3 0.1 reshape.82
  7.4 0.1 fusion.37
  7.5 0.2 reduce_window_sum.11
  7.7 0.2 select_reduce_fusion
  7.9 1.1 fusion.33
  8.9 1.0 fusion.35
  10.0 0.2 broadcast_in_dim.2
  10.1 0.1 reshape.83
  10.3 0.2 convolution_convert_fusion
  10.5 15.5 %all_to_all.10 = bf16[8,1,24,640]{3,2,1,0:T(8,128)(2,1)S(1)} all-to-all(bf16[8,1,24,640]{3,2,1,0:T(8,128)(2,1)S(1)} %bitcast.85), channel_id=1, replica_groups=mesh['ep'=8,'tp'=4] {'ep'}, dimensions={0} | all-to-all | bytes 491520 | tf_op jit(solution)/shard_map/all_to_all | solution.py:34
  26.0 13.9 %all_gather.3 = bf16[8,1,24,2560]{3,2,0,1:T(8,128)(2,1)S(1)} all-gather(bf16[8,1,24,640]{3,2,0,1:T(8,128)(2,1)S(1)} %bitcast.84), channel_id=1, replica_groups=mesh['ep'=8,'tp'=4] {'tp'}, dimensions={3}, use_global_device_ids=true | all-gather | bytes 1228800 | tf_op jit(solution)/shard_map/all_gather | solution.py:35
  39.9 9.2 %fusion.6 = f32[8,1,24,2240]{3,2,0,1:T(8,128)} fusion(bf16[1,2240,2560]{2,1,0:T(8,128)(2,1)} %param.11, bf16[8,1,24,2560]{3,2,0,1:T(8,128)(2,1)S(1)} %all_gather.3), kind=kOutput, calls=%fused_computation.7 | convolution fusion | flops 2202009600 | bytes 14172160 | tf_op jit(solution)/shard_map/sjcd,jfd->sjcf/dot_general | solution.py:36
  49.1 14.7 %fusion.24 = bf16[8,1,24,2560]{3,2,0,1:T(8,128)(2,1)S(1)} fusion(bf16[1,2240,2560]{2,1,0:T(8,128)(2,1)} %param.13, bf16[1,2240,2560]{2,1,0:T(8,128)(2,1)} %param.12, f32[8,1,24,2240]{3,2,0,1:T(8,128)} %fusion.6, bf16[8,1,24,2560]{3,2,0,1:T(8,128)(2,1)S(1)} %all_gather.3), kind=kOutput, calls=%fused_computation.13 | convolution fusion | flops 4407091200 | bytes 26624000 | tf_op jit(solution)/shard_map/sjcf,jfd->sjcd/dot_general | solution.py:39
  63.8 4.6 %copy.20 = bf16[8,1,24,2560]{2,0,1,3:T(8,128)(2,1)} copy(bf16[8,1,24,2560]{3,2,0,1:T(8,128)(2,1)S(1)} %fusion.24) | data formatting | bytes 1966080
  68.4 7.3 %reshape.103 = bf16[2560,192]{1,0:T(8,128)(2,1)} reshape(bf16[2560,1,8,24]{3,2,1,0:T(8,128)(2,1)} %bitcast.81) | data formatting | bytes 1966080
  75.7 28.7 %reduce-scatter.4.cloned.1.call-done = bf16[640,192]{1,0:T(8,128)(2,1)} async-done(((bf16[2560,192]{1,0:T(8,128)(2,1)}), bf16[640,192]{1,0:T(8,128)(2,1)}) %reduce-scatter.4.cloned.1.call-update) | async-done | bytes 245776
  104.5 2.0 %reshape.104 = bf16[640,1,8,24]{3,2,1,0:T(8,128)(2,1)S(1)} reshape(bf16[640,192]{1,0:T(8,128)(2,1)} %reduce-scatter.4.cloned.1.call-done) | data formatting | bytes 491520
  106.5 1.5 %copy.21 = bf16[8,1,24,640]{3,2,0,1:T(8,128)(2,1)} copy(bf16[8,1,24,640]{2,0,1,3:T(8,128)(2,1)S(1)} %bitcast.83) | data formatting | bytes 491520
  108.0 4.6 %all-to-all-start.1 = ((bf16[8,1,24,640]{3,2,1,0:T(8,128)(2,1)}), bf16[8,1,24,640]{3,2,1,0:T(8,128)(2,1)S(1)}, u32[]{:S(2)}, u32[]{:S(2)}) async-start(bf16[8,1,24,640]{3,2,1,0:T(8,128)(2,1)} %bitcast.22), calls=%async_computation.1 | async-start | bytes 491520 | tf_op jit(solution)/shard_map/all_to_all | solution.py:45
  112.7 0.1 mul.78
  112.9 9.0 %all-to-all-done.1 = bf16[8,1,24,640]{3,2,1,0:T(8,128)(2,1)S(1)} async-done(((bf16[8,1,24,640]{3,2,1,0:T(8,128)(2,1)}), bf16[8,1,24,640]{3,2,1,0:T(8,128)(2,1)S(1)}, u32[]{:S(2)}, u32[]{:S(2)}) %all-to-all-start.1) | async-done | bytes 245792 | tf_op jit(solution)/shard_map/all_to_all | solution.py:45
  121.9 0.9 gather_fusion
  122.9 0.9 multiply_reduce_fusion
  (14 shorter events, 0.3 us)
Async XLA Ops:
  6.5 97.9 %reduce-scatter.4.cloned.1.call-start = ((), (), s32[]{:S(2)}) async-start(), calls=%async_computation.3 | async-start | bytes 1638400
  75.7 36.9 %copy-start = (s32[32,4]{0,1:T(4,128)S(1)}, s32[32,4]{0,1:T(4,128)}, u32[]{:S(2)}) copy-start(s32[32,4]{0,1:T(4,128)} %param.9) | copy-start | bytes 1540
  75.7 37.1 %copy-start.1 = (f32[32,4]{0,1:T(4,128)S(1)}, f32[32,4]{0,1:T(4,128)}, u32[]{:S(2)}) copy-start(f32[32,4]{0,1:T(4,128)} %param.10) | copy-start | bytes 1540
  108.0 14.0 %all-to-all-start.1 = ((bf16[8,1,24,640]{3,2,1,0:T(8,128)(2,1)}), bf16[8,1,24,640]{3,2,1,0:T(8,128)(2,1)S(1)}, u32[]{:S(2)}, u32[]{:S(2)}) async-start(bf16[8,1,24,640]{3,2,1,0:T(8,128)(2,1)} %bitcast.22), calls=%async_computation.1 | async-start | bytes 491520 | tf_op jit(solution)/shard_map/all_to_all | solution.py:45
Sparse Core Ops, SparseCore 0:
  75.8 28.5 reduce-scatter.3
where the time goes:
time: 131 us
  waiting for transfers between devices  37.8 us (29%)
  blocking collectives  29.4 us (22%)
  matrix products  24.1 us (18%)
  local copies, waits for them, and re-layouts  17.8 us (14%)
  between operations  13.5 us (10%)
  starting transfers between devices  4.61 us (4%)
  other arithmetic  3.44 us (3%)
    unnamed x2, waiting for transfers between devices  28.8 us
    unnamed x10, local copies, waits for them, and re-layouts  16.2 us
    all_to_all x1, blocking collectives, on_device(): lax.all_to_all(send, 'ep', split_axis=0, concat_axis=0, tiled=True)  15.5 us
    dot_general x1, matrix products, on_device(): jnp.einsum('sjcf,jfd->sjcd', hidden, down_weight, preferred_element_type=...  14.7 us
    all_gather x1, blocking collectives, on_device(): piece = lax.all_gather(arrived, 'tp', axis=3, tiled=True)  13.9 us
    dot_general x1, matrix products, on_device(): jnp.einsum('sjcd,jfd->sjcf', piece, gate_weight, preferred_element_type=j...  9.21 us
    all_to_all x1, waiting for transfers between devices, on_device(): lax.all_to_all(shares, 'ep', split_axis=0, concat_axis=0, tiled=True)  9.04 us
    all_to_all x1, starting transfers between devices, on_device(): lax.all_to_all(shares, 'ep', split_axis=0, concat_axis=0, tiled=True)  4.6 us
  transfers between devices with their start and end apart: 2, of which 2 were waited for; matrix products, arithmetic and copies ran while one was open for 0% of the time, Pallas kernels for 0%

commit v1 on v0

--- a/solution.py
+++ b/solution.py
@@ -1,6 +1,10 @@
+import functools
+
 import jax
 import jax.numpy as jnp
 from jax import lax
+from jax.experimental import pallas as pl
+from jax.experimental.pallas import tpu as pltpu
 from jax.sharding import PartitionSpec as P
 
 epsilon = 1e-06
@@ -48,8 +52,309 @@
     mixed = jnp.sum(route_weight[:, :, None] * picked, axis=1)
     return mixed.astype(jnp.bfloat16)
 
+MESH = pl.DeviceIdType.MESH
+CORES = 2
+F32 = jnp.float32
+BF16 = jnp.bfloat16
+NT = (((1,), (1,)), ((), ()))
+
+
+def row_blocks(total, size):
+    return [(at, min(size, total - at)) for at in range(0, total, size)]
+
+
+def fused(
+    nz, side, tokens_ref, gain_ref, route_ref, weight_ref, gate_hbm, up_hbm, down_hbm, out_ref,
+    wg, wu, wd, xg, acc_g, acc_u, hid, ob, sib, ss, rp, zs, zr, wsend, wrecv,
+    w_sem, z_ssem, z_rsem, own_ssem, own_rsem, f_ssem, f_rsem, t_ssem, t_rsem,
+    r_ssem, r_rsem, s_ssem, s_rsem, x_ssem, x_rsem, y_ssem, y_rsem,
+):
+    ep, tp = lax.axis_index("ep"), lax.axis_index("tp")
+    n_tp, n_ep = side * side, nz * CORES
+    z, core = ep // CORES, ep % CORES
+    ty, tx = tp // side, tp % side
+    rows, width = tokens_ref.shape
+    share = width // n_tp
+    half = nz * rows
+
+    def z_at(dz):
+        return lax.rem(z + dz, nz)
+
+    def from_z(dz):
+        return lax.rem(z + nz - dz, nz)
+
+    def quarter(r):
+        return lax.rem(ty + r // side, side) * side + lax.rem(tx + r % side, side)
+
+    def ep_id(zz, cc):
+        return zz * CORES + cc
+
+    other = 1 - core
+    sibling = ep_id(z, other)
+
+    def part(r):
+        return pl.ds(r * share, share)
+
+    def place(cc, zz):
+        return pl.ds(pl.multiple_of((cc * nz + zz) * rows, rows), rows)
+
+    loads = {}
+    for r in range(n_tp):
+        cols = pl.ds(pl.multiple_of(quarter(r) * share, share), share)
+        for which, (hbm, vmem) in enumerate(((gate_hbm, wg), (up_hbm, wu), (down_hbm, wd))):
+            loads[which, r] = pltpu.make_async_copy(
+                hbm.at[0, :, cols], vmem.at[:, part(r)], w_sem.at[which, r]
+            )
+    for r in range(n_tp):
+        loads[0, r].start()
+        loads[1, r].start()
+    for r in reversed(range(n_tp)):
+        loads[2, r].start()
+
+    barrier = pltpu.get_barrier_semaphore()
+    for step in range(1, n_ep):
+        pl.semaphore_signal(
+            barrier, inc=1, device_id={"ep": lax.rem(ep + step, n_ep)}, device_id_type=MESH
+        )
+    for r in range(1, n_tp):
+        pl.semaphore_signal(barrier, inc=1, device_id={"tp": quarter(r)}, device_id_type=MESH)
+
+    values = tokens_ref[...].astype(F32)
+    scaled = values * lax.rsqrt(jnp.mean(values * values, axis=-1, keepdims=True) + epsilon)
+    normed = (scaled * gain_ref[...]).astype(BF16)
+    for q in range(n_tp):
+        qy, qx = q // side, q % side
+        rel = lax.rem(qy + side - ty, side) * side + lax.rem(qx + side - tx, side)
+        xg[place(core, z), pl.ds(pl.multiple_of(rel * share, share), share)] = normed[
+            :, q * share : (q + 1) * share
+        ]
+    position = (core * nz + z) * rows
+    lanes = lax.broadcasted_iota(jnp.int32, (rows, n_ep * rows), 1)
+    sublanes = lax.broadcasted_iota(jnp.int32, (rows, n_ep * rows), 0)
+    spread = lanes == sublanes + position
+    route, route_weight = route_ref[...], weight_ref[...]
+    for e in range(n_ep):
+        chosen = jnp.sum(jnp.where(route == e, route_weight, 0.0), axis=1, keepdims=True)
+        wsend[e] = jnp.sum(jnp.where(spread, chosen, 0.0), axis=0, keepdims=True)
+    pl.semaphore_wait(barrier, n_ep + n_tp - 2)
+
+    def remote(src, dst, ssem, rsem, target):
+        return pltpu.make_async_remote_copy(
+            src_ref=src, dst_ref=dst, send_sem=ssem, recv_sem=rsem,
+            device_id=target, device_id_type=MESH,
+        )
+
+    sent = []
+
+    def go(copy):
+        copy.start()
+        sent.append(copy)
+        return copy
+
+    z_order = [dz for d in range(1, nz) for dz in ((d, nz - d) if d < nz - d else (d,)) if d <= nz - d]
+    z_copy = {}
+    own = (place(core, z), part(0))
+    for dz in z_order:
+        z_copy[dz] = go(remote(
+            xg.at[own], xg.at[own], z_ssem.at[dz], z_rsem.at[dz], {"ep": ep_id(z_at(dz), core)}
+        ))
+    own_copy = go(remote(
+        xg.at[place(core, z)], xg.at[place(core, z)], own_ssem, own_rsem, {"ep": sibling}
+    ))
+    w_copy = []
+    for step in range(1, n_ep):
+        to = lax.rem(ep + step, n_ep)
+        w_copy.append(go(remote(
+            wsend.at[to], wrecv.at[step], r_ssem.at[step], r_rsem.at[step], {"ep": to}
+        )))
+
+    forward, t_copy = {}, {}
+    for dz in z_order:
+        z_copy[dz].wait_recv()
+        block = (place(core, from_z(dz)), part(0))
+        forward[0, dz] = go(remote(
+            xg.at[block], xg.at[block], f_ssem.at[0, dz], f_rsem.at[0, dz], {"ep": sibling}
+        ))
+        for r in range(1, n_tp - 1):
+            there = (place(core, from_z(dz)), part(r))
+            t_copy[r, dz] = go(remote(
+                xg.at[block], xg.at[there], t_ssem.at[r, dz], t_rsem.at[r, dz], {"tp": quarter(r)}
+            ))
+    for dz in z_order:
+        r = n_tp - 1
+        block, there = (place(core, from_z(dz)), part(0)), (place(core, from_z(dz)), part(r))
+        t_copy[r, dz] = go(remote(
+            xg.at[block], xg.at[there], t_ssem.at[r, dz], t_rsem.at[r, dz], {"tp": quarter(r)}
+        ))
+
+    def pass_on(r):
+        for dz in z_order:
+            t_copy[r, dz].wait_recv()
+            block = (place(core, from_z(dz)), part(r))
+            forward[r, dz] = go(remote(
+                xg.at[block], xg.at[block], f_ssem.at[r, dz], f_rsem.at[r, dz], {"ep": sibling}
+            ))
+
+    def forwarded(r):
+        for dz in z_order:
+            forward[r, dz].wait_recv()
+
+    hidden_rows = wg.shape[0]
+    blocks = row_blocks(hidden_rows, 5 * 128)
+    own_copy.wait_recv()
+    forwarded(0)
+
+    def project(first, last):
+        cols = slice(first * share, last * share)
+        for r in range(first, last):
+            loads[0, r].wait()
+            loads[1, r].wait()
+        held = xg[:, cols]
+        for at, size in blocks:
+            for weights, acc in ((wg, acc_g), (wu, acc_u)):
+                term = lax.dot_general(
+                    weights[at : at + size, cols], held, NT, preferred_element_type=F32
+                )
+                acc[at : at + size, :] = term if first == 0 else acc[at : at + size, :] + term
+
+    project(0, 1)
+    for r in range(1, n_tp - 1):
+        pass_on(r)
+    for r in range(1, n_tp - 1):
+        forwarded(r)
+    project(1, n_tp - 1)
+    pass_on(n_tp - 1)
+    forwarded(n_tp - 1)
+    for copy in w_copy:
+        copy.wait_recv()
+    mix = wsend[ep]
+    for step in range(1, n_ep):
+        mix = mix + wrecv[step]
+    last = n_tp - 1
+    loads[0, last].wait()
+    loads[1, last].wait()
+    cols = slice(last * share, n_tp * share)
+    held = xg[:, cols]
+    for at, size in blocks:
+        gate = acc_g[at : at + size, :] + lax.dot_general(
+            wg[at : at + size, cols], held, NT, preferred_element_type=F32
+        )
+        upward = acc_u[at : at + size, :] + lax.dot_general(
+            wu[at : at + size, cols], held, NT, preferred_element_type=F32
+        )
+        mixed_hidden = (gate / (1.0 + jnp.exp(-gate))) * upward * mix
+        hid[:, at : at + size] = mixed_hidden.T.astype(BF16)
+
+    mine = pl.ds(pl.multiple_of(core * half, half), half)
+    yours = pl.ds(pl.multiple_of(other * half, half), half)
+    back_order = list(reversed(range(n_tp)))
+    far_order = list(reversed(z_order))
+    s_copy, x_copy = {}, {}
+
+    def combine(r):
+        s_copy[r].wait_recv()
+        total = ob[r, mine, :].astype(F32) + sib[r].astype(F32)
+        ss[r] = total.astype(BF16)
+        if r > 0:
+            for dz in far_order + [0]:
+                block = pl.ds(pl.multiple_of(z_at(dz) * rows, rows), rows)
+                x_copy[r, dz] = go(remote(
+                    ss.at[r, block, :], rp.at[r, block, :], x_ssem.at[r, dz], x_rsem.at[r, dz],
+                    {"tp": quarter(r)},
+                ))
+
+    for k, r in enumerate(back_order):
+        loads[2, r].wait()
+        product = jnp.dot(hid[...], wd[:, r * share : (r + 1) * share], preferred_element_type=F32)
+        ob[r] = product.astype(BF16)
+        s_copy[r] = go(remote(
+            ob.at[r, yours, :], sib.at[r], s_ssem.at[r], s_rsem.at[r], {"ep": sibling}
+        ))
+        if k > 0:
+            combine(back_order[k - 1])
+    combine(0)
+    y_copy = {}
+    for dz in far_order + [0]:
+        block = pl.ds(pl.multiple_of(z_at(dz) * rows, rows), rows)
+        total = ss[0, block, :].astype(F32)
+        for r in range(1, n_tp):
+            x_copy[r, dz].wait_recv()
+            total = total + rp[r, block, :].astype(F32)
+        if dz > 0:
+            zs[dz] = total.astype(BF16)
+            y_copy[dz] = go(remote(
+                zs.at[dz], zr.at[dz], y_ssem.at[dz], y_rsem.at[dz], {"ep": ep_id(z_at(dz), core)}
+            ))
+    for dz in far_order:
+        y_copy[dz].wait_recv()
+        total = total + zr[dz].astype(F32)
+    out_ref[...] = total.astype(BF16)
+    for copy in sent:
+        copy.wait_send()
+
+
+def fused_call(nz, side, tokens, norm_gain, route, route_weight, gate_weight, up_weight, down_weight):
+    rows, width = tokens.shape
+    n_tp, n_ep = side * side, nz * CORES
+    share, every, half = width // n_tp, n_ep * rows, nz * rows
+    hidden = gate_weight.shape[1]
+    vmem, dma = pltpu.VMEM, pltpu.SemaphoreType.DMA
+    return pl.pallas_call(
+        functools.partial(fused, nz, side),
+        out_shape=jax.ShapeDtypeStruct((rows, share), BF16),
+        in_specs=[pl.BlockSpec(memory_space=pltpu.VMEM)] * 4
+        + [pl.BlockSpec(memory_space=pl.ANY)] * 3,
+        out_specs=pl.BlockSpec(memory_space=pltpu.VMEM),
+        scratch_shapes=[
+            vmem((hidden, width), BF16),
+            vmem((hidden, width), BF16),
+            vmem((hidden, width), BF16),
+            vmem((every, width), BF16),
+            vmem((hidden, every), F32),
+            vmem((hidden, every), F32),
+            vmem((every, hidden), BF16),
+            vmem((n_tp, every, share), BF16),
+            vmem((n_tp, half, share), BF16),
+            vmem((n_tp, half, share), BF16),
+            vmem((n_tp, half, share), BF16),
+            vmem((nz, rows, share), BF16),
+            vmem((nz, rows, share), BF16),
+            vmem((n_ep, 1, every), F32),
+            vmem((n_ep, 1, every), F32),
+            dma((3, n_tp)),
+            dma((nz,)), dma((nz,)),
+            dma, dma,
+            dma((n_tp, nz)), dma((n_tp, nz)),
+            dma((n_tp, nz)), dma((n_tp, nz)),
+            dma((n_ep,)), dma((n_ep,)),
+            dma((n_tp,)), dma((n_tp,)),
+            dma((n_tp, nz)), dma((n_tp, nz)),
+            dma((nz,)), dma((nz,)),
+        ],
+        compiler_params=pltpu.CompilerParams(
+            collective_id=0, has_side_effects=True, vmem_limit_bytes=60 * 1024 * 1024
+        ),
+    )(tokens, norm_gain[None, :], route, route_weight, gate_weight, up_weight, down_weight)
+
 
 def solution(mesh):
+    n_ep, n_tp = mesh.shape["ep"], mesh.shape["tp"]
+    side = 2
+
+    def body(tokens, norm_gain, route, route_weight, gate_weight, up_weight, down_weight):
+        args = (tokens, norm_gain, route, route_weight, gate_weight, up_weight, down_weight)
+        fits = (
+            n_tp == side * side
+            and n_ep % CORES == 0
+            and gate_weight.shape[0] == 1
+            and tokens.shape[0] % 16 == 0
+            and tokens.shape[1] % (128 * n_tp) == 0
+            and gate_weight.shape[1] % 16 == 0
+        )
+        if fits:
+            return fused_call(n_ep // CORES, side, *args)
+        return on_device(*args)
+
     placed = (
         P("ep", None),
         P(),
@@ -60,5 +365,5 @@
         P("ep", "tp", None),
     )
     return jax.shard_map(
-        on_device, mesh=mesh, in_specs=placed, out_specs=P("ep", "tp"), check_vma=False
-    )
+        body, mesh=mesh, in_specs=placed, out_specs=P("ep", "tp"), check_vma=False
+    )

time: 131 us -> 46.4 us (0.35)
  Pallas kernels: 0 us -> 40.6 us
  waiting for transfers between devices: 37.8 us -> 0 us
  blocking collectives: 29.4 us -> 0 us
  matrix products: 24.1 us -> 0 us
  between operations: 13.5 us -> 0.01 us
  local copies, waits for them, and re-layouts: 17.8 us -> 5.44 us
  starting transfers between devices: 4.61 us -> 0 us
  other arithmetic: 3.44 us -> 0 us
    pallas_call x0 -> x1, Pallas kernels: none -> 40.6 us  [fused_call(): pl.pallas_call(functools.partial(fused, nz, side), out_shape=jax.ShapeDty...]
    unnamed x2 -> x0, waiting for transfers between devices: 28.8 us -> none
    dot_general x3 -> x0, matrix products: 24.1 us -> none  [the longest x1 14.7 us: on_device(): jnp.einsum('sjcf,jfd->sjcd', hidden, down_weight, preferred_element_type=...]
    all_to_all x1 -> x0, blocking collectives: 15.5 us -> none  [on_device(): lax.all_to_all(send, 'ep', split_axis=0, concat_axis=0, tiled=True)]
    all_gather x1 -> x0, blocking collectives: 13.9 us -> none  [on_device(): piece = lax.all_gather(arrived, 'tp', axis=3, tiled=True)]
    unnamed x10 -> x3, local copies, waits for them, and re-layouts: 16.2 us -> 4.13 us
    all_to_all x1 -> x0, waiting for transfers between devices: 9.04 us -> none  [on_device(): lax.all_to_all(shares, 'ep', split_axis=0, concat_axis=0, tiled=True)]
    all_to_all x1 -> x0, starting transfers between devices: 4.6 us -> none  [on_device(): lax.all_to_all(shares, 'ep', split_axis=0, concat_axis=0, tiled=True)]
  transfers between devices with their start and end apart: 2 -> 0, of which waited for: 2 -> 0; matrix products, arithmetic and copies ran while one was open for 0% -> 0% of each run, Pallas kernels for 0% -> 0%
where the time goes in v1:
time: 46.4 us; the launch traced here: 46.1 us
  Pallas kernels  40.6 us (88%)
  local copies, waits for them, and re-layouts  5.44 us (12%)
    pallas_call x1, Pallas kernels, fused_call(): pl.pallas_call(functools.partial(fused, nz, side), out_shape=jax.ShapeDty...  40.6 us
    unnamed x3, local copies, waits for them, and re-layouts  4.13 us
    broadcast_in_dim x1, local copies, waits for them, and re-layouts, fused_call(): norm_gain[None, :]  1.31 us

profile of v1, /device:TPU:0, one launch (start us, length us, event | category | flops | bytes accessed | tf_op | source)
XLA Modules:
  0.0 46.1 jit_solution(834878175467516733)
XLA Ops:
  0.0 1.3 %broadcast_in_dim.3.gain_ref = f32[1,2560]{1,0:T(1,128)} reshape(f32[2560]{0:T(1024)} %param.8) | data formatting | bytes 20480 | tf_op jit(solution)/shard_map/broadcast_in_dim | solution.py:337
  1.3 1.4 %copy.8.route_ref = s32[32,4]{1,0:T(8,128)} copy(s32[32,4]{0,1:T(4,128)} %param.9) | data formatting | bytes 1024 | tf_op args[2]
  2.7 1.4 %copy.9.weight_ref = f32[32,4]{1,0:T(8,128)} copy(f32[32,4]{0,1:T(4,128)} %param.10) | data formatting | bytes 1024 | tf_op args[3]
  4.0 40.6 %shard_map.73 = bf16[32,640]{1,0:T(8,128)(2,1)} custom-call(bf16[32,2560]{1,0:T(8,128)(2,1)} %tokens_ref.1, f32[1,2560]{1,0:T(1,128)} %broadcast_in_dim.3.gain_ref, s32[32,4]{1,0:T(8,128)} %copy.8.route_ref, f32[32,4]{1,0:T(8,128)} %copy.9.weight_ref, bf16[1,2240,2560]{2,1,0:T(8,128)(2,1)} %gate_hbm.1, bf16[1,2240,2560]{2,1,0:T(8,128)(2,1)} %up_hbm.1, ...), custom_call_target="tpu_custom_call" | custom-call | tf_op jit(solution)/shard_map/pallas_call | solution.py:302
  44.7 1.4 %copy.11 = bf16[32,640]{1,0:T(8,128)(2,1)} copy(bf16[32,640]{1,0:T(8,128)(2,1)} %shard_map.73) | data formatting | bytes 81920

commit v2 on v1

--- a/solution.py
+++ b/solution.py
@@ -64,9 +64,9 @@
 
 
 def fused(
-    nz, side, tokens_ref, gain_ref, route_ref, weight_ref, gate_hbm, up_hbm, down_hbm, out_ref,
+    nz, side, tokens_in, gain_in, route_in, weight_in, gate_hbm, up_hbm, down_hbm, out_ref,
     wg, wu, wd, xg, acc_g, acc_u, hid, ob, sib, ss, rp, zs, zr, wsend, wrecv,
-    w_sem, z_ssem, z_rsem, own_ssem, own_rsem, f_ssem, f_rsem, t_ssem, t_rsem,
+    tokens_ref, gain_ref, route_ref, weight_ref, in_sem, w_sem, z_ssem, z_rsem, own_ssem, own_rsem, f_ssem, f_rsem, t_ssem, t_rsem,
     r_ssem, r_rsem, s_ssem, s_rsem, x_ssem, x_rsem, y_ssem, y_rsem,
 ):
     ep, tp = lax.axis_index("ep"), lax.axis_index("tp")
@@ -74,14 +74,25 @@
     z, core = ep // CORES, ep % CORES
     ty, tx = tp // side, tp % side
     rows, width = tokens_ref.shape
+    small = [
+        pltpu.make_async_copy(src, dst, in_sem.at[at])
+        for at, (src, dst) in enumerate((
+            (tokens_in, tokens_ref), (gain_in, gain_ref), (route_in, route_ref), (weight_in, weight_ref),
+        ))
+    ]
+    for copy in small:
+        copy.start()
     share = width // n_tp
     half = nz * rows
 
     def z_at(dz):
-        return lax.rem(z + dz, nz)
-
-    def from_z(dz):
-        return lax.rem(z + nz - dz, nz)
+        at, bit = 0, 1
+        while bit < nz:
+            at = at + lax.rem(z // bit + dz // bit, 2) * bit
+            bit = bit * 2
+        return at
+
+    from_z = z_at
 
     def quarter(r):
         return lax.rem(ty + r // side, side) * side + lax.rem(tx + r % side, side)
@@ -97,6 +108,14 @@
 
     def place(cc, zz):
         return pl.ds(pl.multiple_of((cc * nz + zz) * rows, rows), rows)
+
+    barrier = pltpu.get_barrier_semaphore()
+    for step in range(1, n_ep):
+        pl.semaphore_signal(
+            barrier, inc=1, device_id={"ep": lax.rem(ep + step, n_ep)}, device_id_type=MESH
+        )
+    for r in range(1, n_tp):
+        pl.semaphore_signal(barrier, inc=1, device_id={"tp": quarter(r)}, device_id_type=MESH)
 
     loads = {}
     for r in range(n_tp):
@@ -111,31 +130,27 @@
     for r in reversed(range(n_tp)):
         loads[2, r].start()
 
-    barrier = pltpu.get_barrier_semaphore()
-    for step in range(1, n_ep):
-        pl.semaphore_signal(
-            barrier, inc=1, device_id={"ep": lax.rem(ep + step, n_ep)}, device_id_type=MESH
-        )
-    for r in range(1, n_tp):
-        pl.semaphore_signal(barrier, inc=1, device_id={"tp": quarter(r)}, device_id_type=MESH)
-
+    for copy in small:
+        copy.wait()
     values = tokens_ref[...].astype(F32)
     scaled = values * lax.rsqrt(jnp.mean(values * values, axis=-1, keepdims=True) + epsilon)
-    normed = (scaled * gain_ref[...]).astype(BF16)
+    normed = (scaled * gain_ref[...][None, :]).astype(BF16)
     for q in range(n_tp):
         qy, qx = q // side, q % side
         rel = lax.rem(qy + side - ty, side) * side + lax.rem(qx + side - tx, side)
-        xg[place(core, z), pl.ds(pl.multiple_of(rel * share, share), share)] = normed[
-            :, q * share : (q + 1) * share
-        ]
+        xg[rel, place(core, z), :] = normed[:, q * share : (q + 1) * share]
     position = (core * nz + z) * rows
     lanes = lax.broadcasted_iota(jnp.int32, (rows, n_ep * rows), 1)
     sublanes = lax.broadcasted_iota(jnp.int32, (rows, n_ep * rows), 0)
     spread = lanes == sublanes + position
     route, route_weight = route_ref[...], weight_ref[...]
+    experts = lax.broadcasted_iota(jnp.int32, (n_ep, rows), 0)
+    chosen = jnp.zeros((n_ep, rows), F32)
+    for k in range(route.shape[0]):
+        chosen = chosen + jnp.where(experts == route[k : k + 1], route_weight[k : k + 1], 0.0)
+    chosen = chosen.T
     for e in range(n_ep):
-        chosen = jnp.sum(jnp.where(route == e, route_weight, 0.0), axis=1, keepdims=True)
-        wsend[e] = jnp.sum(jnp.where(spread, chosen, 0.0), axis=0, keepdims=True)
+        wsend[e] = jnp.sum(jnp.where(spread, chosen[:, e : e + 1], 0.0), axis=0, keepdims=True)
     pl.semaphore_wait(barrier, n_ep + n_tp - 2)
 
     def remote(src, dst, ssem, rsem, target):
@@ -151,15 +166,20 @@
         sent.append(copy)
         return copy
 
-    z_order = [dz for d in range(1, nz) for dz in ((d, nz - d) if d < nz - d else (d,)) if d <= nz - d]
+    z_order = list(range(1, nz))
     z_copy = {}
-    own = (place(core, z), part(0))
+    own = (0, place(core, z))
     for dz in z_order:
         z_copy[dz] = go(remote(
             xg.at[own], xg.at[own], z_ssem.at[dz], z_rsem.at[dz], {"ep": ep_id(z_at(dz), core)}
         ))
+    across = (n_tp - 1, place(core, z))
+    t_copy = {(n_tp - 1, 1): go(remote(
+        xg.at[across], xg.at[across], t_ssem.at[n_tp - 1, 1], t_rsem.at[n_tp - 1, 1],
+        {"ep": ep_id(z_at(1), core)},
+    ))}
     own_copy = go(remote(
-        xg.at[place(core, z)], xg.at[place(core, z)], own_ssem, own_rsem, {"ep": sibling}
+        xg.at[:, place(core, z)], xg.at[:, place(core, z)], own_ssem, own_rsem, {"ep": sibling}
     ))
     w_copy = []
     for step in range(1, n_ep):
@@ -168,21 +188,21 @@
             wsend.at[to], wrecv.at[step], r_ssem.at[step], r_rsem.at[step], {"ep": to}
         )))
 
-    forward, t_copy = {}, {}
+    forward = {}
     for dz in z_order:
         z_copy[dz].wait_recv()
-        block = (place(core, from_z(dz)), part(0))
+        block = (0, place(core, from_z(dz)))
         forward[0, dz] = go(remote(
             xg.at[block], xg.at[block], f_ssem.at[0, dz], f_rsem.at[0, dz], {"ep": sibling}
         ))
         for r in range(1, n_tp - 1):
-            there = (place(core, from_z(dz)), part(r))
+            there = (r, place(core, from_z(dz)))
             t_copy[r, dz] = go(remote(
                 xg.at[block], xg.at[there], t_ssem.at[r, dz], t_rsem.at[r, dz], {"tp": quarter(r)}
             ))
-    for dz in z_order:
+    for dz in z_order[1:]:
         r = n_tp - 1
-        block, there = (place(core, from_z(dz)), part(0)), (place(core, from_z(dz)), part(r))
+        block, there = (0, place(core, from_z(dz))), (r, place(core, from_z(dz)))
         t_copy[r, dz] = go(remote(
             xg.at[block], xg.at[there], t_ssem.at[r, dz], t_rsem.at[r, dz], {"tp": quarter(r)}
         ))
@@ -190,7 +210,7 @@
     def pass_on(r):
         for dz in z_order:
             t_copy[r, dz].wait_recv()
-            block = (place(core, from_z(dz)), part(r))
+            block = (r, place(core, from_z(dz)))
             forward[r, dz] = go(remote(
                 xg.at[block], xg.at[block], f_ssem.at[r, dz], f_rsem.at[r, dz], {"ep": sibling}
             ))
@@ -209,7 +229,7 @@
         for r in range(first, last):
             loads[0, r].wait()
             loads[1, r].wait()
-        held = xg[:, cols]
+        held = jnp.concatenate([xg[r] for r in range(first, last)], axis=1)
         for at, size in blocks:
             for weights, acc in ((wg, acc_g), (wu, acc_u)):
                 term = lax.dot_general(
@@ -234,7 +254,7 @@
     loads[0, last].wait()
     loads[1, last].wait()
     cols = slice(last * share, n_tp * share)
-    held = xg[:, cols]
+    held = xg[last]
     for at, size in blocks:
         gate = acc_g[at : at + size, :] + lax.dot_general(
             wg[at : at + size, cols], held, NT, preferred_element_type=F32
@@ -302,14 +322,13 @@
     return pl.pallas_call(
         functools.partial(fused, nz, side),
         out_shape=jax.ShapeDtypeStruct((rows, share), BF16),
-        in_specs=[pl.BlockSpec(memory_space=pltpu.VMEM)] * 4
-        + [pl.BlockSpec(memory_space=pl.ANY)] * 3,
+        in_specs=[pl.BlockSpec(memory_space=pl.ANY)] * 7,
         out_specs=pl.BlockSpec(memory_space=pltpu.VMEM),
         scratch_shapes=[
             vmem((hidden, width), BF16),
             vmem((hidden, width), BF16),
             vmem((hidden, width), BF16),
-            vmem((every, width), BF16),
+            vmem((n_tp, every, share), BF16),
             vmem((hidden, every), F32),
             vmem((hidden, every), F32),
             vmem((every, hidden), BF16),
@@ -321,6 +340,11 @@
             vmem((nz, rows, share), BF16),
             vmem((n_ep, 1, every), F32),
             vmem((n_ep, 1, every), F32),
+            vmem(tokens.shape, BF16),
+            vmem(norm_gain.shape, F32),
+            vmem(route.T.shape, jnp.int32),
+            vmem(route.T.shape, F32),
+            dma((4,)),
             dma((3, n_tp)),
             dma((nz,)), dma((nz,)),
             dma, dma,
@@ -334,7 +358,7 @@
         compiler_params=pltpu.CompilerParams(
             collective_id=0, has_side_effects=True, vmem_limit_bytes=60 * 1024 * 1024
         ),
-    )(tokens, norm_gain[None, :], route, route_weight, gate_weight, up_weight, down_weight)
+    )(tokens, norm_gain, route.T, route_weight.T, gate_weight, up_weight, down_weight)
 
 
 def solution(mesh):
@@ -346,6 +370,8 @@
         fits = (
             n_tp == side * side
             and n_ep % CORES == 0
+            and n_ep // CORES > 1
+            and (n_ep // CORES) & (n_ep // CORES - 1) == 0
             and gate_weight.shape[0] == 1
             and tokens.shape[0] % 16 == 0
             and tokens.shape[1] % (128 * n_tp) == 0

time: 46.4 us -> 40.9 us (0.88)
  local copies, waits for them, and re-layouts: 5.44 us -> 1.4 us
  Pallas kernels: 40.6 us -> 39.3 us
    unnamed x3 -> x1, local copies, waits for them, and re-layouts: 4.13 us -> 1.4 us
    broadcast_in_dim x1 -> x0, local copies, waits for them, and re-layouts: 1.31 us -> none  [fused_call(): norm_gain[None, :]]
    pallas_call x1, Pallas kernels: 40.6 us -> 39.3 us  [fused_call(): pl.pallas_call(functools.partial(fused, nz, side), out_shape=jax.ShapeDty...]
where the time goes in v2:
time: 40.9 us; the launch traced here: 40.7 us
  Pallas kernels  39.3 us (96%)
  local copies, waits for them, and re-layouts  1.4 us (3%)
    pallas_call x1, Pallas kernels, fused_call(): pl.pallas_call(functools.partial(fused, nz, side), out_shape=jax.ShapeDty...  39.3 us
    unnamed x1, local copies, waits for them, and re-layouts  1.4 us

profile of v2, /device:TPU:0, one launch (start us, length us, event | category | flops | bytes accessed | tf_op | source)
XLA Modules:
  0.0 40.7 jit_solution(4890975710217596013)
XLA Ops:
  0.0 39.3 %shard_map.73 = bf16[32,640]{1,0:T(8,128)(2,1)} custom-call(bf16[32,2560]{1,0:T(8,128)(2,1)} %tokens_in.1, f32[2560]{0:T(1024)} %gain_in.1, s32[4,32]{1,0:T(4,128)} %bitcast.2, f32[4,32]{1,0:T(4,128)} %bitcast.3, bf16[1,2240,2560]{2,1,0:T(8,128)(2,1)} %gate_hbm.1, bf16[1,2240,2560]{2,1,0:T(8,128)(2,1)} %up_hbm.1, bf16[1,2240,2560]{2,1,0:T(8,128)(2,1)} %down_hbm.1), custom_call_target="tpu_custom_call" | custom-call | tf_op jit(solution)/shard_map/pallas_call | solution.py:322
  39.3 1.4 %copy.9 = bf16[32,640]{1,0:T(8,128)(2,1)} copy(bf16[32,640]{1,0:T(8,128)(2,1)} %shard_map.73) | data formatting | bytes 81920
